TPU v7x, 32 devices: a whole 2x2x4 slice. The times are simulated.
32 devices in a mesh: grp: 2 (over y), sp: 4 (over z), tp: 4 (over x, core).
Axes of the slice: x: 2, y: 2, z: 4, core: 2. Of those that a mesh axis runs over, the one named last changes fastest.
Arguments:
- tokens: bfloat16 [4096, 2, 2048], P(('grp', 'sp', 'tp')), parts along dimension 0, may hold values from -64 to 64
- w_query: bfloat16 [2048, 2048], P(None, 'tp'), may hold values from -0.21875 to 0.21875
- w_key: bfloat16 [2048, 2048], P(None, 'tp'), may hold values from -0.125 to 0.125
- w_value: bfloat16 [2048, 2048], P(None, 'tp'), may hold values from -0.125 to 0.125
- w_out: bfloat16 [2048, 2048], P('tp'), may hold values from -0.125 to 0.125
- head_lambda: float32 [16], P('tp'), may hold values from 0.3 to 0.8
- sub_gain: float32 [128], replicated, may hold values from 0.1 to 1.9
Outputs:
- mixed: bfloat16 [4096, 2, 2048], P(('grp', 'sp', 'tp')), parts along dimension 0
There are 2 independent parts, one for each index of `grp`. A program takes and returns all parts, laid end to end along the dimension named above; an argument that names none is the same for every part. Nothing has to cross between parts.
All inputs are finite; a program needn't handle non-finite values.
Results may differ from a plain program's by a relative error of at most 0.015.
The roundings to bfloat16 on the way count: a program that leaves them out, or rounds other values in their place, can miss the bound.
Values may be sent and summed in bfloat16 or wider, within the bound.
No kernel may reach another device: no remote copies, remote signals or barrier semaphores. Data moves between devices by JAX's collectives and lax.ppermute only.
A program may use at most 128 MiB of HBM per device.

v0:
```python
import math

import jax
import jax.numpy as jnp
from jax import lax
from jax.sharding import PartitionSpec as P

SPAN = 64


NEG_FILL = -1e30
EPS_NORM = 1e-06


def key_block(state_in, queries, query_pos, key_blk, value_blk, key_start):
    run_max, run_sum, run_acc = state_in
    blk_len = key_blk.shape[0]
    heads_here = queries.shape[1]
    head_dim = queries.shape[3]
    key_pos = key_start + jnp.arange(blk_len, dtype=jnp.int32)
    key_four = key_blk.reshape(blk_len, heads_here, 2, head_dim)
    scores = jnp.einsum("qhmd,khmd->mhqk", queries, key_four, preferred_element_type=jnp.float32)
    scores = scores * head_dim ** (-0.5)
    allowed = (key_pos // SPAN)[None, :] <= (query_pos // SPAN)[:, None]
    new_max = jnp.maximum(run_max, jnp.max(jnp.where(allowed, scores, NEG_FILL), axis=-1))
    expo_vals = jnp.where(allowed, jnp.exp(scores - new_max[..., None]), 0.0)
    factor = jnp.exp(run_max - new_max)
    run_sum = run_sum * factor + jnp.sum(expo_vals, axis=-1)
    value_three = value_blk.reshape(blk_len, heads_here, 2 * head_dim)
    mixed_vals = jnp.einsum(
        "mhqk,khe->mhqe",
        expo_vals.astype(jnp.bfloat16),
        value_three,
        preferred_element_type=jnp.float32,
    )
    run_acc = run_acc * factor[..., None] + mixed_vals
    return (new_max, run_sum, run_acc)


def guarded_block(state_in, queries, query_pos, key_blk, value_blk, key_start):
    last_pos = query_pos[-1]

    def compute(inner_state):
        return key_block(inner_state, queries, query_pos, key_blk, value_blk, key_start)

    def keep(inner_state):
        return inner_state

    return lax.cond(key_start <= last_pos, compute, keep, state_in)


def sequence_piece(state_in, queries, query_pos, key_part, value_part):
    length = key_part.shape[0]
    step_len = math.gcd(length, 512)
    step_count = length // step_len

    def one_step(step_index, inner_state):
        offset = step_index * step_len
        key_blk = lax.dynamic_slice_in_dim(key_part, offset, step_len, 0)
        value_blk = lax.dynamic_slice_in_dim(value_part, offset, step_len, 0)
        return guarded_block(inner_state, queries, query_pos, key_blk, value_blk, offset)

    return lax.fori_loop(0, step_count, one_step, state_in)


def normalize(attn, sub_gain):
    mean_sq = jnp.mean(attn * attn, axis=-1, keepdims=True)
    normed = (attn * lax.rsqrt(mean_sq + EPS_NORM) * sub_gain).astype(jnp.bfloat16)
    return jnp.transpose(normed, (1, 0, 2)).reshape(attn.shape[1], attn.shape[0] * attn.shape[2])


def on_device(tokens, w_query, w_key, w_value, w_out, head_lambda, sub_gain):
    tp_count = lax.axis_size("tp")
    tok_rows = tokens.shape[0] * tp_count
    seq_count = tokens.shape[1]
    heads_here = head_lambda.shape[0]
    head_dim = w_query.shape[1] // (2 * heads_here)
    value_dim = 2 * head_dim
    query_cols = w_query.shape[1]
    w_joined = jnp.concatenate([w_query, w_key, w_value], axis=1)
    joined = jnp.dot(
        lax.all_gather(tokens, "tp", axis=0, tiled=True),
        w_joined,
        preferred_element_type=jnp.float32,
    ).astype(jnp.bfloat16)
    query_flat = joined[:, :, :query_cols]
    keys_here = joined[:, :, query_cols : 2 * query_cols]
    values_here = joined[:, :, 2 * query_cols :]
    sp_index = lax.axis_index("sp")
    own_first = sp_index * tok_rows
    lam_col = head_lambda[:, None, None]

    def attend(query_sets, first_rows):
        positions = [first + jnp.arange(tok_rows, dtype=jnp.int32) for first in first_rows]
        query_four = [qset.reshape(tok_rows, heads_here, 2, head_dim) for qset in query_sets]
        start_one = (
            jnp.full((2, heads_here, tok_rows), NEG_FILL, jnp.float32),
            jnp.zeros((2, heads_here, tok_rows), jnp.float32),
            jnp.zeros((2, heads_here, tok_rows, value_dim), jnp.float32),
        )
        start_state = tuple((start_one for seq_index in range(seq_count)))
        key_part = lax.all_gather(keys_here, "sp", axis=0, tiled=True)
        value_part = lax.all_gather(values_here, "sp", axis=0, tiled=True)
        new_states = []
        for seq_index in range(seq_count):
            new_states.append(
                sequence_piece(
                    start_state[seq_index],
                    query_four[seq_index],
                    positions[seq_index],
                    key_part[:, seq_index],
                    value_part[:, seq_index],
                )
            )
        final_states = tuple(new_states)
        results = []
        for run_max, run_sum, run_acc in final_states:
            attn = run_acc[0] / run_sum[0][..., None] - lam_col * run_acc[1] / run_sum[1][..., None]
            results.append(normalize(attn, sub_gain))
        return results

    normed_list = attend(
        [query_flat[:, seq_index] for seq_index in range(seq_count)],
        [own_first for seq_index in range(seq_count)],
    )
    normed = jnp.stack(normed_list, axis=1)
    return lax.psum_scatter(
        jnp.dot(normed, w_out, preferred_element_type=jnp.float32).astype(jnp.bfloat16),
        "tp",
        scatter_dimension=0,
        tiled=True,
    )


def solution(mesh):
    return jax.shard_map(
        on_device,
        mesh=mesh,
        in_specs=(
            P(("grp", "sp", "tp"), None, None),
            P(None, "tp"),
            P(None, "tp"),
            P(None, "tp"),
            P("tp", None),
            P("tp"),
            P(),
        ),
        out_specs=P(("grp", "sp", "tp"), None, None),
        check_vma=False,
    )
```

profile of v0, /device:TPU:0, one launch (start us, length us, event | category | flops | bytes accessed | tf_op | source)
XLA Modules:
  0.0 373.5 jit_solution(4716763115918646867)
XLA Ops:
  6.5 2.7 copy.39
  9.3 4.0 %copy.36 = bf16[2048,512]{0,1:T(8,128)(2,1)} copy(bf16[2048,512]{1,0:T(8,128)(2,1)} %param.16) | data formatting | bytes 4194304 | tf_op args[1]
  13.3 4.0 %copy.37 = bf16[2048,512]{0,1:T(8,128)(2,1)} copy(bf16[2048,512]{1,0:T(8,128)(2,1)} %param.17) | data formatting | bytes 4194304 | tf_op args[2]
  17.3 4.1 %copy.38 = bf16[2048,512]{0,1:T(8,128)(2,1)} copy(bf16[2048,512]{1,0:T(8,128)(2,1)} %param.18) | data formatting | bytes 4194304 | tf_op args[3]
  21.4 25.2 %all-gather.4.cloned.1.call-done = bf16[512,2,2048]{2,0,1:T(8,128)(2,1)} async-done(((bf16[128,2,2048]{2,0,1:T(8,128)(2,1)}), bf16[512,2,2048]{2,0,1:T(8,128)(2,1)}) %all-gather.4.cloned.1.call-update) | async-done | bytes 4194320 | tf_op jit(solution)/shard_map/all_gather | solution.py:82
  46.6 10.8 %fusion.38 = bf16[512,2,1536]{0,2,1:T(8,128)(2,1)S(1)} fusion(bf16[512,2,2048]{2,0,1:T(8,128)(2,1)} %all-gather.4.cloned.1.call-done, bf16[2048,512]{0,1:T(8,128)(2,1)} %copy.38, bf16[2048,512]{0,1:T(8,128)(2,1)} %copy.37, bf16[2048,512]{0,1:T(8,128)(2,1)} %copy.36), kind=kOutput, calls=%fused_computation.74 | convolution fusion | flops 6462898176 | bytes 13631488 | tf_op jit(solution)/shard_map/dot_general | solution.py:81
  57.4 1.7 copy-done.5
  59.1 1.5 fusion.57
  62.9 78.6 %all-gather.6.cloned.1.call-done = bf16[2048,2,512]{0,2,1:T(8,128)(2,1)} async-done(((bf16[512,2,512]{0,2,1:T(8,128)(2,1)}), bf16[2048,2,512]{0,2,1:T(8,128)(2,1)}) %all-gather.6.cloned.1.call-update) | async-done | bytes 4194320 | tf_op jit(solution)/shard_map/all_gather | solution.py:102
  141.5 4.8 %slice_bitcast_fusion.3 = (bf16[2048,512]{0,1:T(8,128)(2,1)}, bf16[2048,512]{0,1:T(8,128)(2,1)}) fusion(bf16[2048,2,512]{0,2,1:T(8,128)(2,1)} %all-gather.6.cloned.1.call-done), kind=kLoop, calls=%fused_computation.78 | loop fusion | bytes 8388608 | tf_op jit(solution)/shard_map/squeeze | solution.py:111
  146.3 76.0 %all-gather.8.cloned.1.call-done = bf16[2048,2,512]{0,2,1:T(8,128)(2,1)} async-done(((bf16[512,2,512]{0,2,1:T(8,128)(2,1)}), bf16[2048,2,512]{0,2,1:T(8,128)(2,1)}) %all-gather.8.cloned.1.call-update) | async-done | bytes 4194320 | tf_op jit(solution)/shard_map/all_gather | solution.py:103
  222.3 4.8 %slice_bitcast_fusion.2 = (bf16[2048,512]{0,1:T(8,128)(2,1)}, bf16[2048,512]{0,1:T(8,128)(2,1)}) fusion(bf16[2048,2,512]{0,2,1:T(8,128)(2,1)} %all-gather.8.cloned.1.call-done), kind=kLoop, calls=%fused_computation.77 | loop fusion | bytes 8388608 | tf_op jit(solution)/shard_map/squeeze | solution.py:112
  227.2 1.5 broadcast_in_dim.64.clone.1
  228.7 13.6 %while.35 = (s32[]{:T(128)}, f32[2,4,512]{2,1,0:T(4,128)S(1)}, f32[2,4,512]{2,1,0:T(4,128)S(1)}, f32[2,4,512,128]{3,2,0,1:T(8,128)}, s32[512]{0:T(512)S(1)}, /*i...) while((s32[]{:T(128)}, f32[2,4,512]{2,1,0:T(4,128)S(1)}, ...), condition=%wide.region_12.13_spmd, body=%wide.region_7.12_spmd.sunk | while | flops 823418368 | bytes 50882912 | solution.py:63
  229.9 8.5 %conditional.5 = ((f32[2,4,512]{2,1,0:T(4,128)S(1)}, f32[2,4,512]{2,1,0:T(4,128)S(1)}, f32[2,4,512,128]{3,2,0,1:T(8,128)})) conditional(s32[]{:T(128)} %convert_element_type.61, (f32[2,4,512]{2,1,0:T(4,128)S(1)}, f32[2,4,512]{2,1,0:T(4,128)S(1)}, f32[2,4,512,128]{3,2,0,1:T(8,128)}) %tuple.117, (s32[]{:T(128)}, s32[512]{0:T(512)S(1)}, ...), branch_computations={%region_8.8_spmd, %region_9.0_spmd} | conditional | flops 823418368 | bytes 50882692 | solution.py:49
  229.9 1.3 constant_dynamic-slice_fusion.2
  231.5 1.5 fusion.16
  233.0 2.0 fusion.19
  235.0 2.0 bitcast_add_fusion.1
  237.1 1.3 copy-done.4
  242.2 1.6 broadcast_in_dim.64.clone
  243.8 13.6 %while.34 = (s32[]{:T(128)}, f32[2,4,512]{2,1,0:T(4,128)S(1)}, f32[2,4,512]{2,1,0:T(4,128)S(1)}, f32[2,4,512,128]{3,2,0,1:T(8,128)}, s32[512]{0:T(512)S(1)}, /*i...) while((s32[]{:T(128)}, f32[2,4,512]{2,1,0:T(4,128)S(1)}, ...), condition=%wide.region_5.6_spmd, body=%wide.region_0.5_spmd.sunk | while | flops 823418368 | bytes 50882912 | solution.py:63
  245.1 8.5 %conditional.4 = ((f32[2,4,512]{2,1,0:T(4,128)S(1)}, f32[2,4,512]{2,1,0:T(4,128)S(1)}, f32[2,4,512,128]{3,2,0,1:T(8,128)})) conditional(s32[]{:T(128)} %convert_element_type.60, (f32[2,4,512]{2,1,0:T(4,128)S(1)}, f32[2,4,512]{2,1,0:T(4,128)S(1)}, f32[2,4,512,128]{3,2,0,1:T(8,128)}) %tuple.114, (s32[]{:T(128)}, s32[512]{0:T(512)S(1)}, ...), branch_computations={%region_1.0_spmd, %region_2.4_spmd} | conditional | flops 823418368 | bytes 50882692 | solution.py:49
  245.1 1.3 constant_dynamic-slice_fusion
  246.6 1.5 fusion
  248.2 2.0 fusion.3
  250.2 2.0 bitcast_add_fusion
  252.2 1.4 copy-done.2
  257.5 4.0 %multiply_reduce_fusion.1 = (f32[4,512]{1,0:T(4,128)S(1)}, f32[4,512,128]{2,1,0:T(8,128)S(1)}, f32[4,512]{1,0:T(4,128)S(1)}, f32[4,512,128]{2,1,0:T(8,128)S(1)}) fusion(f32[4,512]{1,0:T(4,128)S(1)} %get-tuple-element.612, f32[4]{0:T(128)S(1)} %copy-done.6, f32[4,512]{1,0:T(4,128)S(1)} %get-tuple-element.611, f32[4,512]{1,0:T(4,128)S(1)} %get-tuple-element.614, ...), kind=kLoop, calls=%fused_computation.97 | loop fusion | flops 3141632 | bytes 6340624 | tf_op jit(solution)/shard_map/reduce_sum | solution.py:67
  264.5 5.3 %convolution_convert_fusion = bf16[512,2,2048]{2,0,1:T(8,128)(2,1)} fusion(bf16[512,2048]{1,0:T(8,128)(2,1)S(1)} %copy-done, bf16[512,1,512]{2,0,1:T(8,128)(2,1)S(1)} %stack_reshape.7, bf16[512,1,512]{2,0,1:T(8,128)(2,1)} %stack_reshape.6), kind=kOutput, calls=%fused_computation.73 | convolution fusion | flops 2150105088 | bytes 7340032 | tf_op jit(solution)/shard_map/dot_general | solution.py:128
  269.9 93.8 %reduce-scatter.2.cloned.1.call-done = bf16[128,2,2048]{2,0,1:T(8,128)(2,1)} async-done(((bf16[512,2,2048]{2,0,1:T(8,128)(2,1)}), bf16[128,2,2048]{2,0,1:T(8,128)(2,1)}) %reduce-scatter.2.cloned.1.call-update) | async-done | bytes 1048592 | tf_op jit(solution)/shard_map/reduce_scatter | solution.py:127
  363.7 3.3 copy.47
  (63 shorter events, 10.8 us)
Async XLA Ops:
  6.5 258.0 %copy-start = (bf16[512,2048]{1,0:T(8,128)(2,1)S(1)}, bf16[512,2048]{1,0:T(8,128)(2,1)}, u32[]{:S(2)}) copy-start(bf16[512,2048]{1,0:T(8,128)(2,1)} %param.19) | copy-start | bytes 6291460
  6.5 40.1 %all-gather.4.cloned.1.call-start = ((), (), s32[]{:S(2)}) async-start(), calls=%async_computation.1 | async-start | bytes 5242880 | tf_op jit(solution)/shard_map/all_gather | solution.py:82
  9.3 132.2 %all-gather.6.cloned.1.call-start = ((), (), s32[]{:S(2)}) async-start(), calls=%async_computation.2 | async-start | bytes 5242880 | tf_op jit(solution)/shard_map/all_gather | solution.py:102
  57.4 1.7 copy-start.5
  60.6 161.7 %all-gather.8.cloned.1.call-start = ((), (), s32[]{:S(2)}) async-start(), calls=%async_computation.3 | async-start | bytes 5242880 | tf_op jit(solution)/shard_map/all_gather | solution.py:103
  61.3 302.4 %reduce-scatter.2.cloned.1.call-start = ((), (), s32[]{:S(2)}) async-start(), calls=%async_computation.4 | async-start | bytes 5242880 | tf_op jit(solution)/shard_map/reduce_scatter | solution.py:127
  233.0 2.0 copy-start.3
  237.0 1.3 copy-start.4
  243.8 13.7 %copy-start.6 = (f32[4]{0:T(128)S(1)}, f32[4]{0:T(128)}, u32[]{:S(2)}) copy-start(f32[4]{0:T(128)} %param.20) | copy-start | bytes 52
  248.1 2.0 copy-start.1
  252.2 1.4 copy-start.2
  257.5 4.0 %copy-start.7 = (f32[128]{0:T(128)S(1)}, f32[128]{0:T(128)}, u32[]{:S(2)}) copy-start(f32[128]{0:T(128)} %param.21) | copy-start | bytes 1540
Sparse Core Ops, SparseCore 0:
  9.4 37.1 all-gather.3
  60.7 80.7 all-gather.5
  143.1 79.2 all-gather.7
  270.0 93.6 reduce-scatter.1
where the time goes:
time: 374 us
  waiting for transfers between devices  274 us (73%)
  local copies, waits for them, and re-layouts  47.4 us (13%)
  matrix products  23.2 us (6%)
  between operations  13.3 us (4%)
  other arithmetic  9.39 us (3%)
  loops' own time  5.57 us (1%)
    reduce_scatter x1, waiting for transfers between devices, on_device(): lax.psum_scatter(jnp.dot(normed, w_out, preferred_element_type=jnp.float3...  93.8 us
    all_gather x1, waiting for transfers between devices, attend(): key_part = lax.all_gather(keys_here, 'sp', axis=0, tiled=True)  78.6 us
    all_gather x1, waiting for transfers between devices, attend(): value_part = lax.all_gather(values_here, 'sp', axis=0, tiled=True)  76 us
    all_gather x1, waiting for transfers between devices, on_device(): lax.all_gather(tokens, 'tp', axis=0, tiled=True)  25.2 us
    unnamed x12, local copies, waits for them, and re-layouts  16.5 us
    dot_general x1, matrix products, on_device(): jnp.dot(lax.all_gather(tokens, 'tp', axis=0, tiled=True), w_joined, prefe...  10.8 us
  transfers between devices with their start and end apart: 4, of which 4 were waited for; matrix products, arithmetic and copies ran while one was open for 5% of the time, Pallas kernels for 0%

commit v1 on v0

--- a/solution.py
+++ b/solution.py
@@ -1,8 +1,11 @@
+import functools
 import math
 
 import jax
 import jax.numpy as jnp
 from jax import lax
+from jax.experimental import pallas as pl
+from jax.experimental.pallas import tpu as pltpu
 from jax.sharding import PartitionSpec as P
 
 SPAN = 64
@@ -10,6 +13,7 @@
 
 NEG_FILL = -1e30
 EPS_NORM = 1e-06
+VMEM_LIMIT = 60 * 1024 * 1024
 
 
 def key_block(state_in, queries, query_pos, key_blk, value_blk, key_start):
@@ -69,7 +73,7 @@
     return jnp.transpose(normed, (1, 0, 2)).reshape(attn.shape[1], attn.shape[0] * attn.shape[2])
 
 
-def on_device(tokens, w_query, w_key, w_value, w_out, head_lambda, sub_gain):
+def gathered_plan(tokens, w_query, w_key, w_value, w_out, head_lambda, sub_gain):
     tp_count = lax.axis_size("tp")
     tok_rows = tokens.shape[0] * tp_count
     seq_count = tokens.shape[1]
@@ -132,6 +136,312 @@
     )
 
 
+ANY = pl.BlockSpec(memory_space=pl.ANY)
+VMEM = pl.BlockSpec(memory_space=pltpu.VMEM)
+SMEM = pl.BlockSpec(memory_space=pltpu.SMEM)
+
+
+def project_kernel(pieces, ids, *refs):
+    piece_refs = refs[:pieces]
+    w_query, w_key, w_value, out_ref, rows_buf, sems = refs[pieces:]
+    piece_rows = piece_refs[0].shape[0]
+    cols = out_ref.shape[1] // 3
+    me = ids[1]
+    copies = []
+    for index in range(pieces):
+        start = pl.multiple_of((me ^ index) * piece_rows, piece_rows)
+        copies.append(
+            pltpu.make_async_copy(piece_refs[index], rows_buf.at[pl.ds(start, piece_rows)], sems.at[index])
+        )
+    for copy in copies:
+        copy.start()
+    for copy in copies:
+        copy.wait()
+    for index, w_ref in enumerate((w_query, w_key, w_value)):
+        out_ref[:, index * cols : (index + 1) * cols] = jnp.dot(
+            rows_buf[...], w_ref[...], preferred_element_type=jnp.float32
+        ).astype(jnp.bfloat16)
+
+
+def project(ids, pieces, w_query, w_key, w_value, cols):
+    count = len(pieces)
+    piece_rows, depth = pieces[0].shape
+    rows = count * piece_rows
+    w_spec = pl.BlockSpec((depth, cols), lambda step, ids: (0, ids[0]))
+    return pl.pallas_call(
+        functools.partial(project_kernel, count),
+        grid_spec=pltpu.PrefetchScalarGridSpec(
+            num_scalar_prefetch=1,
+            grid=(1,),
+            in_specs=[ANY] * count + [w_spec] * 3,
+            out_specs=pl.BlockSpec((rows, 3 * cols), lambda step, ids: (0, 0)),
+            scratch_shapes=[
+                pltpu.VMEM((rows, depth), jnp.bfloat16),
+                pltpu.SemaphoreType.DMA((count,)),
+            ],
+        ),
+        out_shape=jax.ShapeDtypeStruct((rows, 3 * cols), jnp.bfloat16),
+        compiler_params=pltpu.CompilerParams(vmem_limit_bytes=VMEM_LIMIT),
+        cost_estimate=pl.CostEstimate(
+            flops=2 * rows * depth * 3 * cols,
+            bytes_accessed=2 * (rows * depth + 3 * depth * cols + 3 * rows * cols),
+            transcendentals=0,
+        ),
+        name="project",
+    )(ids, *pieces, w_query, w_key, w_value)
+
+
+def attend_kernel(shards, parts, tile, ids, *refs):
+    chunk_refs = refs[:shards]
+    lam_ref, gain_ref = refs[shards : shards + 2]
+    outs = refs[shards + 2 : shards + 2 + shards * parts // 2]
+    qkv_buf, score_buf, out_buf, sems, out_sems = refs[shards + 2 + shards * parts // 2 :]
+    rows = chunk_refs[0].shape[0]
+    length = qkv_buf.shape[0]
+    cols = qkv_buf.shape[1] // 3
+    value_dim = gain_ref.shape[1]
+    heads = cols // value_dim
+    head_dim = value_dim // 2
+    piece_rows = rows // parts
+    z_here, t_here = ids[2], ids[1]
+    copies = []
+    for index in range(shards):
+        start = pl.multiple_of((z_here ^ index) * rows, rows)
+        copies.append(
+            pltpu.make_async_copy(chunk_refs[index], qkv_buf.at[pl.ds(start, rows)], sems.at[index])
+        )
+    for copy in copies:
+        copy.start()
+    for copy in copies:
+        copy.wait()
+
+    lanes = lax.broadcasted_iota(jnp.int32, (tile, value_dim), 1)
+    first_map = lanes < head_dim
+    ones = jnp.ones((tile, value_dim), jnp.bfloat16)
+    span_q = lax.broadcasted_iota(jnp.int32, (2 * tile, tile), 0) % tile // SPAN
+    span_k = lax.broadcasted_iota(jnp.int32, (2 * tile, tile), 1) // SPAN
+    allowed = span_k <= span_q
+    scale = head_dim ** (-0.5)
+
+    @pl.loop(0, heads)
+    def one_head(head):
+        def lane_slab(base):
+            return pl.ds(pl.multiple_of(base + head * value_dim, value_dim), value_dim)
+
+        lam = lam_ref[head]
+        for q_tile in range(length // tile):
+            q_rows = pl.ds(q_tile * tile, tile)
+            query = qkv_buf[q_rows, lane_slab(0)] * jnp.bfloat16(scale)
+            zero = jnp.zeros_like(query)
+            both = jnp.concatenate(
+                [jnp.where(first_map, query, zero), jnp.where(first_map, zero, query)], axis=0
+            )
+            top = None
+            for k_tile in range(q_tile + 1):
+                key = qkv_buf[pl.ds(k_tile * tile, tile), lane_slab(cols)]
+                scores = lax.dot_general(
+                    both, key, (((1,), (1,)), ((), ())), preferred_element_type=jnp.float32
+                )
+                if k_tile == q_tile:
+                    scores = jnp.where(allowed, scores, NEG_FILL)
+                score_buf[:, k_tile * tile : (k_tile + 1) * tile] = scores
+                tile_top = functools.reduce(
+                    jnp.maximum,
+                    [scores[:, c : c + 128] for c in range(0, tile, 128)],
+                )
+                top = tile_top if top is None else jnp.maximum(top, tile_top)
+            top = jnp.max(top, axis=1, keepdims=True)
+            acc = None
+            for k_tile in range(q_tile + 1):
+                scores = score_buf[:, k_tile * tile : (k_tile + 1) * tile]
+                expo = jnp.exp(scores - top).astype(jnp.bfloat16)
+                value = qkv_buf[pl.ds(k_tile * tile, tile), lane_slab(2 * cols)]
+                term = jnp.dot(
+                    expo, jnp.concatenate([value, ones], axis=1), preferred_element_type=jnp.float32
+                )
+                acc = term if acc is None else acc + term
+            ratio = acc[:, :value_dim] / acc[:, value_dim:]
+            attn = ratio[:tile] - lam * ratio[tile:]
+            mean_sq = jnp.mean(attn * attn, axis=1, keepdims=True)
+            normed = (attn * lax.rsqrt(mean_sq + EPS_NORM) * gain_ref[...]).astype(jnp.bfloat16)
+            for piece in range(tile // piece_rows):
+                block = q_tile * (tile // piece_rows) + piece
+                shard, part = block // parts, block % parts
+                other = part ^ t_here
+                out_buf[
+                    z_here ^ shard,
+                    other & 1,
+                    other >> 1,
+                    :,
+                    lane_slab(0),
+                ] = normed[piece * piece_rows : (piece + 1) * piece_rows]
+
+    out_copies = []
+    for index, out_ref in enumerate(outs):
+        out_copies.append(
+            pltpu.make_async_copy(out_buf.at[index // 2, index % 2], out_ref, out_sems.at[index])
+        )
+    for copy in out_copies:
+        copy.start()
+    for copy in out_copies:
+        copy.wait()
+
+
+def attend(ids, chunks, lam_here, gain, parts):
+    shards = len(chunks)
+    rows, all_cols = chunks[0].shape
+    length = shards * rows
+    cols = all_cols // 3
+    value_dim = gain.shape[1]
+    heads = cols // value_dim
+    piece_rows = rows // parts
+    tile = 2 * piece_rows
+    n_out = shards * parts // 2
+    out_shape = jax.ShapeDtypeStruct((2, piece_rows, cols), jnp.bfloat16)
+    scored = heads * 2 * length * (length + tile) // 2
+    return pl.pallas_call(
+        functools.partial(attend_kernel, shards, parts, tile),
+        in_specs=[SMEM] + [ANY] * shards + [SMEM, VMEM],
+        out_specs=[ANY] * n_out,
+        out_shape=[out_shape] * n_out,
+        scratch_shapes=[
+            pltpu.VMEM((length, all_cols), jnp.bfloat16),
+            pltpu.VMEM((2 * tile, length), jnp.float32),
+            pltpu.VMEM((shards, 2, parts // 2, piece_rows, cols), jnp.bfloat16),
+            pltpu.SemaphoreType.DMA((shards,)),
+            pltpu.SemaphoreType.DMA((n_out,)),
+        ],
+        compiler_params=pltpu.CompilerParams(vmem_limit_bytes=VMEM_LIMIT),
+        cost_estimate=pl.CostEstimate(
+            flops=2 * scored * 4 * value_dim,
+            bytes_accessed=2 * length * (all_cols + cols),
+            transcendentals=scored,
+        ),
+        name="attend",
+    )(ids, *chunks, lam_here, gain)
+
+
+def mix_kernel(shards, side, ids, *refs):
+    n_in = 2 * shards
+    w_own, w_near, out_ref, rows_buf, sems = refs[n_in:]
+    in_refs = refs[:n_in]
+    piece_rows, cols = in_refs[0].shape[1:]
+    z_here = ids[2]
+    half, low = z_here // 2, z_here % 2
+
+    @pl.when(pl.program_id(0) == 0)
+    def load_rows():
+        copies = []
+        for index, in_ref in enumerate(in_refs):
+            z_xor, t_xor = index // 2, index % 2
+            seq = half ^ (z_xor // 2)
+            row = pl.multiple_of(seq * piece_rows, piece_rows)
+            lane = pl.multiple_of((low ^ (z_xor % 2)) * cols + 2 * t_xor * cols, cols)
+            copies.append(
+                pltpu.make_async_copy(
+                    in_ref.at[side],
+                    rows_buf.at[pl.ds(row, piece_rows), pl.ds(lane, cols)],
+                    sems.at[index],
+                )
+            )
+        for copy in copies:
+            copy.start()
+        for copy in copies:
+            copy.wait()
+
+    own_depth = w_own.shape[0]
+    out_ref[...] = (
+        jnp.dot(rows_buf[:, :own_depth], w_own[...], preferred_element_type=jnp.float32)
+        + jnp.dot(rows_buf[:, own_depth:], w_near[...], preferred_element_type=jnp.float32)
+    ).astype(out_ref.dtype)
+
+
+def mix(ids, parts_in, w_own, w_near, side, out_dtype):
+    shards = len(parts_in) // 2
+    piece_rows, cols = parts_in[0].shape[1:]
+    depth, width = w_own.shape
+    rows = 2 * piece_rows
+    block = min(width, 512)
+    return pl.pallas_call(
+        functools.partial(mix_kernel, shards, side),
+        grid_spec=pltpu.PrefetchScalarGridSpec(
+            num_scalar_prefetch=1,
+            grid=(width // block,),
+            in_specs=[ANY] * len(parts_in)
+            + [pl.BlockSpec((depth, block), lambda step, ids: (0, step))] * 2,
+            out_specs=pl.BlockSpec((rows, block), lambda step, ids: (0, step)),
+            scratch_shapes=[
+                pltpu.VMEM((rows, 2 * depth), jnp.bfloat16),
+                pltpu.SemaphoreType.DMA((len(parts_in),)),
+            ],
+        ),
+        out_shape=jax.ShapeDtypeStruct((rows, width), out_dtype),
+        compiler_params=pltpu.CompilerParams(vmem_limit_bytes=VMEM_LIMIT),
+        cost_estimate=pl.CostEstimate(
+            flops=4 * rows * depth * width,
+            bytes_accessed=2 * (2 * rows * depth + 2 * depth * width + rows * width),
+            transcendentals=0,
+        ),
+        name=f"mix_{side}",
+    )(ids, *parts_in, w_own, w_near)
+
+
+def swap(value, axis, distance):
+    size = lax.axis_size(axis)
+    return lax.ppermute(value, axis, [(index, index ^ distance) for index in range(size)])
+
+
+def swap_both(value, z_xor, t_xor):
+    sp, tp = lax.axis_size("sp"), lax.axis_size("tp")
+    pairs = [
+        (z * tp + t, (z ^ z_xor) * tp + (t ^ t_xor)) for z in range(sp) for t in range(tp)
+    ]
+    return lax.ppermute(value, ("sp", "tp"), pairs)
+
+
+def split_plan(tokens, w_query, w_key, w_value, w_out, head_lambda, sub_gain):
+    z_here = lax.axis_index("sp")
+    t_here = lax.axis_index("tp")
+    tp = lax.axis_size("tp")
+    half, low = z_here // 2, z_here % 2
+    heads_mine = head_lambda.shape[0] // 2
+    cols = w_query.shape[1] // 2
+    ids = jnp.stack([low, t_here, z_here]).astype(jnp.int32)
+    own = lax.dynamic_index_in_dim(tokens, half, 1, keepdims=False)
+    away = lax.dynamic_index_in_dim(tokens, 1 - half, 1, keepdims=False)
+    far = swap(away, "sp", 2)
+    near = swap(own, "sp", 1)
+    far_near = swap(far, "sp", 1)
+    w_near = swap(w_out, "tp", 1)
+    chunks = []
+    for piece in (own, near, far, far_near):
+        crossed = swap(piece, "tp", 2)
+        pieces = [piece, swap(piece, "tp", 1), crossed, swap(crossed, "tp", 1)]
+        chunks.append(project(ids, pieces, w_query, w_key, w_value, cols))
+    lam_here = lax.dynamic_slice_in_dim(head_lambda, low * heads_mine, heads_mine, 0)
+    outs = attend(ids, chunks, lam_here, sub_gain[None, :], tp)
+    received = [outs[0]]
+    for index in range(1, len(outs)):
+        received.append(swap_both(outs[index], index // 2, index % 2))
+    partial = swap(mix(ids, received, w_out, w_near, 1, jnp.bfloat16), "tp", 2)
+    kept = mix(ids, received, w_out, w_near, 0, jnp.float32)
+    total = (kept + partial.astype(jnp.float32)).astype(jnp.bfloat16)
+    return jnp.transpose(total.reshape(2, tokens.shape[0], total.shape[1]), (1, 0, 2))
+
+
+def on_device(tokens, w_query, w_key, w_value, w_out, head_lambda, sub_gain):
+    seqs = tokens.shape[1]
+    sp, tp = lax.axis_size("sp"), lax.axis_size("tp")
+    heads_here = head_lambda.shape[0]
+    lane_heads = w_query.shape[1] // heads_here % 128 == 0
+    whole_tiles = tokens.shape[0] % 128 == 0
+    if seqs == 2 and sp == 4 and tp == 4 and heads_here % 2 == 0 and lane_heads and whole_tiles:
+        plan = split_plan
+    else:
+        plan = gathered_plan
+    return plan(tokens, w_query, w_key, w_value, w_out, head_lambda, sub_gain)
+
+
 def solution(mesh):
     return jax.shard_map(
         on_device,

time: 374 us -> 176 us (0.47)
  waiting for transfers between devices: 274 us -> 79.8 us
  Pallas kernels: 0 us -> 59.2 us
  local copies, waits for them, and re-layouts: 47.4 us -> 8.65 us
  matrix products: 23.2 us -> 0 us
  starting transfers between devices: 0.3 us -> 22.5 us
  between operations: 13.3 us -> 0.28 us
  other arithmetic: 9.39 us -> 2.46 us
  loops' own time: 5.57 us -> 0 us
    all_gather x3 -> x0, waiting for transfers between devices: 180 us -> none  [the longest x1 78.6 us: attend(): key_part = lax.all_gather(keys_here, 'sp', axis=0, tiled=True)]
    reduce_scatter x1 -> x0, waiting for transfers between devices: 93.8 us -> none  [on_device(): lax.psum_scatter(jnp.dot(normed, w_out, preferred_element_type=jnp.float3...]
    ppermute x0 -> x24, waiting for transfers between devices: none -> 79.8 us  [the longest x17 64.1 us: swap(): lax.ppermute(value, axis, [(index, index ^ distance) for index in range(s...]
    pallas_call x0 -> x7, Pallas kernels: none -> 59.2 us  [the longest x4 27 us: project(): pl.pallas_call(functools.partial(project_kernel, count), grid_spec=pltpu....]
    dot_general x6 -> x0, matrix products: 23.2 us -> none  [the longest x1 10.8 us: on_device(): jnp.dot(lax.all_gather(tokens, 'tp', axis=0, tiled=True), w_joined, prefe...]
    ppermute x0 -> x24, starting transfers between devices: none -> 22.5 us  [the longest x17 15.2 us: swap(): lax.ppermute(value, axis, [(index, index ^ distance) for index in range(s...]
    unnamed x12 -> x36, local copies, waits for them, and re-layouts: 16.5 us -> 2.15 us
    squeeze x2 -> x0, local copies, waits for them, and re-layouts: 9.62 us -> none  [the longest x1 4.83 us: attend(): value_part[:, seq_index]]
  transfers between devices with their start and end apart: 4 -> 24, of which waited for: 4 -> 9; matrix products, arithmetic and copies ran while one was open for 5% -> 1% of each run, Pallas kernels for 0% -> 30%
where the time goes in v1:
time: 176 us; the launch traced here: 173 us
  waiting for transfers between devices  79.8 us (45%)
  Pallas kernels  59.2 us (34%)
  starting transfers between devices  22.5 us (13%)
  local copies, waits for them, and re-layouts  8.65 us (5%)
  other arithmetic  2.46 us (1%)
    ppermute x17, waiting for transfers between devices, swap(): lax.ppermute(value, axis, [(index, index ^ distance) for index in range(s...  64.1 us
    pallas_call x4, Pallas kernels, project(): pl.pallas_call(functools.partial(project_kernel, count), grid_spec=pltpu....  27 us
    pallas_call x1, Pallas kernels, attend(): pl.pallas_call(functools.partial(attend_kernel, shards, parts, tile), in_...  18.8 us
    ppermute x7, waiting for transfers between devices, swap_both(): return lax.ppermute(value, ('sp', 'tp'), pairs)  15.7 us
    ppermute x17, starting transfers between devices, swap(): lax.ppermute(value, axis, [(index, index ^ distance) for index in range(s...  15.2 us
    pallas_call x2, Pallas kernels, mix(): pl.pallas_call(functools.partial(mix_kernel, shards, side), grid_spec=plt...  13.4 us
    ppermute x7, starting transfers between devices, swap_both(): return lax.ppermute(value, ('sp', 'tp'), pairs)  7.32 us
    dynamic_slice x1, local copies, waits for them, and re-layouts, split_plan(): away = lax.dynamic_index_in_dim(tokens, 1 - half, 1, keepdims=False)  3.8 us
  transfers between devices with their start and end apart: 24, of which 9 were waited for; matrix products, arithmetic and copies ran while one was open for 1% of the time, Pallas kernels for 30%

profile of v1, /device:TPU:0, one launch (start us, length us, event | category | flops | bytes accessed | tf_op | source)
XLA Modules:
  0.0 172.9 jit_solution(16345561841237857807)
XLA Ops:
  0.0 3.8 %constant_dynamic-slice_fusion = (bf16[128,1,2048]{2,1,0:T(2,128)(2,1)S(1)}, bf16[128,1,2048]{2,1,0:T(2,128)(2,1)S(1)}) fusion(bf16[128,2,2048]{2,1,0:T(2,128)(2,1)} %param.7, s32[]{:T(128)S(6)} %select_n.24, s32[]{:T(128)S(6)} %select_n.23), kind=kLoop, calls=%fused_computation.5 | loop fusion | bytes 2097160 | tf_op jit(solution)/shard_map/jit(dynamic_index_in_dim)/dynamic_slice | solution.py:411
  4.1 3.1 %collective-permute-start.3 = (bf16[128,2048]{1,0:T(8,128)(2,1)S(1)}, bf16[128,2048]{1,0:T(8,128)(2,1)S(1)}, u32[]{:S(2)}, u32[]{:S(2)}) collective-permute-start(bf16[128,2048]{1,0:T(8,128)(2,1)S(1)} %bitcast.15), channel_id=1, source_target_pairs={{0,4},{4,0},{8,12},{12,8},{1,5},{5,1},{9,13},{13,9},{2,6},{6,2},{1... | collective-permute-start | bytes 1572872 | tf_op jit(solution)/shard_map/ppermute | solution.py:391
  7.6 2.7 %collective-permute-start.7 = (bf16[128,2048]{1,0:T(8,128)(2,1)S(1)}, bf16[128,2048]{1,0:T(8,128)(2,1)S(1)}, u32[]{:S(2)}, u32[]{:S(2)}) collective-permute-start(bf16[128,2048]{1,0:T(8,128)(2,1)S(1)} %bitcast.19), channel_id=1, source_target_pairs={{0,8},{4,12},{8,0},{12,4},{1,9},{5,13},{9,1},{13,5},{2,10},{6,14},... | collective-permute-start | bytes 1572872 | tf_op jit(solution)/shard_map/ppermute | solution.py:391
  10.2 1.5 collective-permute-start.1
  11.7 18.2 %collective-permute-done.3.refs_0_ = bf16[128,2048]{1,0:T(8,128)(2,1)S(1)} collective-permute-done((bf16[128,2048]{1,0:T(8,128)(2,1)S(1)}, bf16[128,2048]{1,0:T(8,128)(2,1)S(1)}, u32[]{:S(2)}, u32[]{:S(2)}) %collective-permute-start.3) | collective-permute-done | bytes 524320 | tf_op jit(solution)/shard_map/ppermute | solution.py:391
  29.9 1.7 collective-permute-start.5
  31.6 1.6 collective-permute-done.7.refs_0_
  33.8 1.5 collective-permute-start.9
  35.3 9.5 %collective-permute-done.5.refs_2_ = bf16[128,2048]{1,0:T(8,128)(2,1)} collective-permute-done((bf16[128,2048]{1,0:T(8,128)(2,1)S(1)}, bf16[128,2048]{1,0:T(8,128)(2,1)}, u32[]{:S(2)}, u32[]{:S(2)}) %collective-permute-start.5) | collective-permute-done | bytes 524320 | tf_op jit(solution)/shard_map/ppermute | solution.py:391
  44.9 1.7 collective-permute-start.13
  47.1 9.0 %collective-permute-done.9.refs_2_ = bf16[128,2048]{1,0:T(8,128)(2,1)} collective-permute-done((bf16[128,2048]{1,0:T(8,128)(2,1)S(1)}, bf16[128,2048]{1,0:T(8,128)(2,1)}, u32[]{:S(2)}, u32[]{:S(2)}) %collective-permute-start.9) | collective-permute-done | bytes 524320 | tf_op jit(solution)/shard_map/ppermute | solution.py:391
  56.2 0.7 dynamic_slice.12.refs_4_
  57.3 8.3 %collective-permute-done.13.refs_2_ = bf16[128,2048]{1,0:T(8,128)(2,1)} collective-permute-done((bf16[128,2048]{1,0:T(8,128)(2,1)}, bf16[128,2048]{1,0:T(8,128)(2,1)}, u32[]{:S(2)}, u32[]{:S(2)}) %collective-permute-start.13) | collective-permute-done | bytes 524320 | tf_op jit(solution)/shard_map/ppermute | solution.py:391
  66.2 6.7 %project.4.refs_0_ = bf16[512,768]{1,0:T(8,128)(2,1)} custom-call(s32[3]{0:T(128)} %pad_add_fusion.ids, bf16[128,2048]{1,0:T(8,128)(2,1)} %bitcast.18, bf16[128,2048]{1,0:T(8,128)(2,1)} %copy-done.5, bf16[128,2048]{1,0:T(8,128)(2,1)} %copy-done.4, bf16[128,2048]{1,0:T(8,128)(2,1)} %copy-done.7, bf16[2048,512]{1,0:T(8,128)(2,1)} %refs_4_.7, ...), custom_call_target="tpu_custom_call" | custom-call | flops 1610612736 | bytes 6029312 | tf_op jit(solution)/shard_map/project/pallas_call | solution.py:171
  73.0 6.8 %project.5.refs_1_ = bf16[512,768]{1,0:T(8,128)(2,1)} custom-call(s32[3]{0:T(128)} %pad_add_fusion.ids, bf16[128,2048]{1,0:T(8,128)(2,1)} %copy-done.3, bf16[128,2048]{1,0:T(8,128)(2,1)} %copy-done.6, bf16[128,2048]{1,0:T(8,128)(2,1)} %collective-permute-done.5.refs_2_, bf16[128,2048]{1,0:T(8,128)(2,1)} %collective-permute-done.6.refs_3_, ...), custom_call_target="tpu_custom_call" | custom-call | flops 1610612736 | bytes 6029312 | tf_op jit(solution)/shard_map/project/pallas_call | solution.py:171
  79.8 6.8 %project.6.refs_2_ = bf16[512,768]{1,0:T(8,128)(2,1)} custom-call(s32[3]{0:T(128)} %pad_add_fusion.ids, bf16[128,2048]{1,0:T(8,128)(2,1)} %copy-done.2, bf16[128,2048]{1,0:T(8,128)(2,1)} %collective-permute-done.8.refs_1_, bf16[128,2048]{1,0:T(8,128)(2,1)} %collective-permute-done.9.refs_2_, bf16[128,2048]{1,0:T(8,128)(2,1)} %collective-permute-done.10.refs_3_, ...), custom_call_target="tpu_custom_call" | custom-call | flops 1610612736 | bytes 6029312 | tf_op jit(solution)/shard_map/project/pallas_call | solution.py:171
  86.5 0.8 copy-done.8
  87.3 6.8 %project.7.refs_3_ = bf16[512,768]{1,0:T(8,128)(2,1)} custom-call(s32[3]{0:T(128)} %pad_add_fusion.ids, bf16[128,2048]{1,0:T(8,128)(2,1)} %collective-permute-done.11.refs_0_, bf16[128,2048]{1,0:T(8,128)(2,1)} %copy-done.8, bf16[128,2048]{1,0:T(8,128)(2,1)} %collective-permute-done.13.refs_2_, bf16[128,2048]{1,0:T(8,128)(2,1)} %collective-permute-done.14.refs_3_, ...), custom_call_target="tpu_custom_call" | custom-call | flops 1610612736 | bytes 6029312 | tf_op jit(solution)/shard_map/project/pallas_call | solution.py:171
  94.1 18.8 %attend.1 = (bf16[2,128,256]{2,1,0:T(8,128)(2,1)}, bf16[2,128,256]{2,1,0:T(8,128)(2,1)}, bf16[2,128,256]{2,1,0:T(8,128)(2,1)}, bf16[2,128,256]{2,1,0:T(8,128)(2,...) custom-call(s32[3]{0:T(128)} %pad_add_fusion.ids, ...), custom_call_target="tpu_custom_call" | custom-call | flops 9663676416 | bytes 4194304 | tf_op jit(solution)/shard_map/attend/pallas_call | solution.py:302
  113.5 1.4 collective-permute-start.17
  114.9 1.5 collective-permute-start.18
  116.4 1.5 collective-permute-start.19
  117.9 2.4 %collective-permute-start.20 = (bf16[2,128,256]{2,1,0:T(8,128)(2,1)}, bf16[2,128,256]{2,1,0:T(8,128)(2,1)S(1)}, u32[]{:S(2)}, u32[]{:S(2)}) collective-permute-start(bf16[2,128,256]{2,1,0:T(8,128)(2,1)} %get-tuple-element.19), channel_id=1, source_target_pairs={{0,12},{1,13},{2,14},{3,15},{4,8},{5,9},{6,10},{7,11},{8,4},{9,5},... | collective-permute-start | bytes 393224 | tf_op jit(solution)/shard_map/ppermute | solution.py:399
  120.2 3.1 %collective-permute-done.16.refs_2_ = bf16[2,128,256]{2,1,0:T(8,128)(2,1)S(1)} collective-permute-done((bf16[2,128,256]{2,1,0:T(8,128)(2,1)}, bf16[2,128,256]{2,1,0:T(8,128)(2,1)S(1)}, u32[]{:S(2)}, u32[]{:S(2)}) %collective-permute-start.16) | collective-permute-done | bytes 131104 | tf_op jit(solution)/shard_map/ppermute | solution.py:399
  123.4 1.0 collective-permute-done.17.refs_3_
  124.4 11.6 %collective-permute-done.19.refs_5_ = bf16[2,128,256]{2,1,0:T(8,128)(2,1)S(1)} collective-permute-done((bf16[2,128,256]{2,1,0:T(8,128)(2,1)}, bf16[2,128,256]{2,1,0:T(8,128)(2,1)S(1)}, u32[]{:S(2)}, u32[]{:S(2)}) %collective-permute-start.19) | collective-permute-done | bytes 131104 | tf_op jit(solution)/shard_map/ppermute | solution.py:399
  136.8 6.6 %mix_1.1 = bf16[256,2048]{1,0:T(8,128)(2,1)} custom-call(s32[3]{0:T(128)} %pad_add_fusion.ids, bf16[2,128,256]{2,1,0:T(8,128)(2,1)} %get-tuple-element.13.refs_0_, bf16[2,128,256]{2,1,0:T(8,128)(2,1)} %copy-done.9, bf16[2,128,256]{2,1,0:T(8,128)(2,1)} %copy-done.10, bf16[2,128,256]{2,1,0:T(8,128)(2,1)} %copy-done.11, bf16[2,128,256]{2,1,0:T(8,128)(2,1)} %copy-done.12, ...), custom_call_target="tpu_custom_call" | custom-call | flops 1073741824 | bytes 5767168 | tf_op jit(solution)/shard_map/mix_1/pallas_call | solution.py:365
  143.3 1.4 collective-permute-start.23
  144.8 6.8 %mix_0.1 = f32[256,2048]{1,0:T(8,128)} custom-call(s32[3]{0:T(128)} %pad_add_fusion.ids, bf16[2,128,256]{2,1,0:T(8,128)(2,1)} %get-tuple-element.13.refs_0_, bf16[2,128,256]{2,1,0:T(8,128)(2,1)} %copy-done.9, bf16[2,128,256]{2,1,0:T(8,128)(2,1)} %copy-done.10, bf16[2,128,256]{2,1,0:T(8,128)(2,1)} %copy-done.11, bf16[2,128,256]{2,1,0:T(8,128)(2,1)} %copy-done.12, ...), custom_call_target="tpu_custom_call" | custom-call | flops 1073741824 | bytes 5767168 | tf_op jit(solution)/shard_map/mix_0/pallas_call | solution.py:365
  151.6 17.4 %collective-permute-done.23 = bf16[256,2048]{1,0:T(8,128)(2,1)S(1)} collective-permute-done((bf16[256,2048]{1,0:T(8,128)(2,1)}, bf16[256,2048]{1,0:T(8,128)(2,1)S(1)}, u32[]{:S(2)}, u32[]{:S(2)}) %collective-permute-start.23) | collective-permute-done | bytes 1048608 | tf_op jit(solution)/shard_map/ppermute | solution.py:391
  169.0 1.9 %add_convert_fusion = bf16[256,2048]{1,0:T(8,128)(2,1)S(1)} fusion(f32[256,2048]{1,0:T(8,128)} %mix_0.1, bf16[256,2048]{1,0:T(8,128)(2,1)S(1)} %collective-permute-done.23), kind=kLoop, calls=%fused_computation | loop fusion | flops 1572864 | bytes 4194304 | tf_op jit(solution)/shard_map/convert_element_type | solution.py:428
  170.9 2.1 %copy.17 = bf16[2,128,2048]{2,0,1:T(2,128)(2,1)} copy(bf16[2,128,2048]{2,1,0:T(8,128)(2,1)S(1)} %bitcast.14) | data formatting | bytes 2097152 | tf_op jit(solution)/shard_map/reshape | solution.py:429
  (64 shorter events, 4.3 us)
Async XLA Ops:
  3.8 42.7 %copy-start = (bf16[512,2048]{1,0:T(8,128)(2,1)S(1)}, bf16[512,2048]{1,0:T(8,128)(2,1)}, u32[]{:S(2)}) copy-start(bf16[512,2048]{1,0:T(8,128)(2,1)} %refs_8_.3) | copy-start | bytes 6291460
  3.8 52.4 %copy-start.16 = (f32[4]{0:T(128)S(1)}, f32[4]{0:T(128)}, u32[]{:S(2)}) copy-start(f32[4]{0:T(128)} %param.12) | copy-start | bytes 52
  4.1 62.1 %copy-start.1 = (bf16[128,1,2048]{2,0,1:T(8,128)(2,1)}, bf16[128,1,2048]{2,0,1:T(8,128)(2,1)S(1)}, u32[]{:S(2)}) copy-start(bf16[128,1,2048]{2,0,1:T(8,128)(2,1)S(1)} %copy.19) | copy-start | bytes 1572868
  4.1 25.8 %collective-permute-start.3 = (bf16[128,2048]{1,0:T(8,128)(2,1)S(1)}, bf16[128,2048]{1,0:T(8,128)(2,1)S(1)}, u32[]{:S(2)}, u32[]{:S(2)}) collective-permute-start(bf16[128,2048]{1,0:T(8,128)(2,1)S(1)} %bitcast.15), channel_id=1, source_target_pairs={{0,4},{4,0},{8,12},{12,8},{1,5},{5,1},{9,13},{13,9},{2,6},{6,2},{1... | collective-permute-start | bytes 1572872 | tf_op jit(solution)/shard_map/ppermute | solution.py:391
  7.6 25.6 %collective-permute-start.7 = (bf16[128,2048]{1,0:T(8,128)(2,1)S(1)}, bf16[128,2048]{1,0:T(8,128)(2,1)S(1)}, u32[]{:S(2)}, u32[]{:S(2)}) collective-permute-start(bf16[128,2048]{1,0:T(8,128)(2,1)S(1)} %bitcast.19), channel_id=1, source_target_pairs={{0,8},{4,12},{8,0},{12,4},{1,9},{5,13},{9,1},{13,5},{2,10},{6,14},... | collective-permute-start | bytes 1572872 | tf_op jit(solution)/shard_map/ppermute | solution.py:391
  10.2 23.1 %collective-permute-start.1 = (bf16[128,2048]{1,0:T(8,128)(2,1)S(1)}, bf16[128,2048]{1,0:T(8,128)(2,1)S(1)}, u32[]{:S(2)}, u32[]{:S(2)}) collective-permute-start(bf16[128,2048]{1,0:T(8,128)(2,1)S(1)} %bitcast.16), channel_id=1, source_target_pairs={{0,2},{1,3},{2,0},{3,1},{4,6},{5,7},{6,4},{7,5},{8,10},{9,11},{10,... | collective-permute-start | bytes 1572872 | tf_op jit(solution)/shard_map/ppermute | solution.py:391
  11.7 22.1 %collective-permute-start = (bf16[128,2048]{1,0:T(8,128)(2,1)S(1)}, bf16[128,2048]{1,0:T(8,128)(2,1)S(1)}, u32[]{:S(2)}, u32[]{:S(2)}) collective-permute-start(bf16[128,2048]{1,0:T(8,128)(2,1)S(1)} %bitcast.17), channel_id=1, source_target_pairs={{0,1},{1,0},{2,3},{3,2},{4,5},{5,4},{6,7},{7,6},{8,9},{9,8},{10,11... | collective-permute-start | bytes 1572872 | tf_op jit(solution)/shard_map/ppermute | solution.py:391
  29.9 26.1 %copy-start.3 = (bf16[128,2048]{1,0:T(8,128)(2,1)}, bf16[128,2048]{1,0:T(8,128)(2,1)S(1)}, u32[]{:S(2)}) copy-start(bf16[128,2048]{1,0:T(8,128)(2,1)S(1)} %collective-permute-done.3.refs_0_) | copy-start | bytes 1572868
  29.9 14.9 %collective-permute-start.5 = (bf16[128,2048]{1,0:T(8,128)(2,1)S(1)}, bf16[128,2048]{1,0:T(8,128)(2,1)}, u32[]{:S(2)}, u32[]{:S(2)}) collective-permute-start(bf16[128,2048]{1,0:T(8,128)(2,1)S(1)} %collective-permute-done.3.refs_0_), channel_id=1, source_target_pairs={{0,2},{1,3},{2,0},{3,1},{4,6},{5,7},{6,4},{7,5},{8,10},{9,11},{10,... | collective-permute-start | bytes 1572872 | tf_op jit(solution)/shard_map/ppermute | solution.py:391
  33.2 39.7 %copy-start.2 = (bf16[128,2048]{1,0:T(8,128)(2,1)}, bf16[128,2048]{1,0:T(8,128)(2,1)S(1)}, u32[]{:S(2)}) copy-start(bf16[128,2048]{1,0:T(8,128)(2,1)S(1)} %collective-permute-done.7.refs_0_) | copy-start | bytes 1572868
  33.2 11.6 %collective-permute-start.11 = (bf16[128,2048]{1,0:T(8,128)(2,1)S(1)}, bf16[128,2048]{1,0:T(8,128)(2,1)}, u32[]{:S(2)}, u32[]{:S(2)}) collective-permute-start(bf16[128,2048]{1,0:T(8,128)(2,1)S(1)} %collective-permute-done.7.refs_0_), channel_id=1, source_target_pairs={{0,4},{4,0},{8,12},{12,8},{1,5},{5,1},{9,13},{13,9},{2,6},{6,2},{1... | collective-permute-start | bytes 1572872 | tf_op jit(solution)/shard_map/ppermute | solution.py:391
  33.3 13.2 %collective-permute-start.4 = (bf16[128,2048]{1,0:T(8,128)(2,1)S(1)}, bf16[128,2048]{1,0:T(8,128)(2,1)S(1)}, u32[]{:S(2)}, u32[]{:S(2)}) collective-permute-start(bf16[128,2048]{1,0:T(8,128)(2,1)S(1)} %collective-permute-done.3.refs_0_), channel_id=1, source_target_pairs={{0,1},{1,0},{2,3},{3,2},{4,5},{5,4},{6,7},{7,6},{8,9},{9,8},{10,11... | collective-permute-start | bytes 1572872 | tf_op jit(solution)/shard_map/ppermute | solution.py:391
  33.3 22.8 %copy-start.4 = (bf16[128,2048]{1,0:T(8,128)(2,1)}, bf16[128,2048]{1,0:T(8,128)(2,1)S(1)}, u32[]{:S(2)}) copy-start(bf16[128,2048]{1,0:T(8,128)(2,1)S(1)} %collective-permute-done.1.refs_2_) | copy-start | bytes 1572868
  33.3 13.5 %collective-permute-start.2 = (bf16[128,2048]{1,0:T(8,128)(2,1)S(1)}, bf16[128,2048]{1,0:T(8,128)(2,1)S(1)}, u32[]{:S(2)}, u32[]{:S(2)}) collective-permute-start(bf16[128,2048]{1,0:T(8,128)(2,1)S(1)} %collective-permute-done.1.refs_2_), channel_id=1, source_target_pairs={{0,1},{1,0},{2,3},{3,2},{4,5},{5,4},{6,7},{7,6},{8,9},{9,8},{10,11... | collective-permute-start | bytes 1572872 | tf_op jit(solution)/shard_map/ppermute | solution.py:391
  33.8 22.3 %copy-start.5 = (bf16[128,2048]{1,0:T(8,128)(2,1)}, bf16[128,2048]{1,0:T(8,128)(2,1)S(1)}, u32[]{:S(2)}) copy-start(bf16[128,2048]{1,0:T(8,128)(2,1)S(1)} %collective-permute-done.refs_1_) | copy-start | bytes 1572868
  33.8 22.3 %collective-permute-start.9 = (bf16[128,2048]{1,0:T(8,128)(2,1)S(1)}, bf16[128,2048]{1,0:T(8,128)(2,1)}, u32[]{:S(2)}, u32[]{:S(2)}) collective-permute-start(bf16[128,2048]{1,0:T(8,128)(2,1)S(1)} %collective-permute-done.7.refs_0_), channel_id=1, source_target_pairs={{0,2},{1,3},{2,0},{3,1},{4,6},{5,7},{6,4},{7,5},{8,10},{9,11},{10,... | collective-permute-start | bytes 1572872 | tf_op jit(solution)/shard_map/ppermute | solution.py:391
  44.8 12.0 %collective-permute-start.6 = (bf16[128,2048]{1,0:T(8,128)(2,1)}, bf16[128,2048]{1,0:T(8,128)(2,1)}, u32[]{:S(2)}, u32[]{:S(2)}) collective-permute-start(bf16[128,2048]{1,0:T(8,128)(2,1)} %collective-permute-done.5.refs_2_), channel_id=1, source_target_pairs={{0,1},{1,0},{2,3},{3,2},{4,5},{5,4},{6,7},{7,6},{8,9},{9,8},{10,11... | collective-permute-start | bytes 1572872 | tf_op jit(solution)/shard_map/ppermute | solution.py:391
  44.9 20.8 %collective-permute-start.13 = (bf16[128,2048]{1,0:T(8,128)(2,1)}, bf16[128,2048]{1,0:T(8,128)(2,1)}, u32[]{:S(2)}, u32[]{:S(2)}) collective-permute-start(bf16[128,2048]{1,0:T(8,128)(2,1)} %collective-permute-done.11.refs_0_), channel_id=1, source_target_pairs={{0,2},{1,3},{2,0},{3,1},{4,6},{5,7},{6,4},{7,5},{8,10},{9,11},{10,... | collective-permute-start | bytes 1572872 | tf_op jit(solution)/shard_map/ppermute | solution.py:391
  46.5 69.9 %collective-permute-start.22 = (bf16[512,2048]{1,0:T(8,128)(2,1)S(1)}, bf16[512,2048]{1,0:T(8,128)(2,1)}, u32[]{:S(2)}, u32[]{:S(2)}) collective-permute-start(bf16[512,2048]{1,0:T(8,128)(2,1)S(1)} %copy-done), channel_id=1, source_target_pairs={{0,1},{1,0},{2,3},{3,2},{4,5},{5,4},{6,7},{7,6},{8,9},{9,8},{10,11... | collective-permute-start | bytes 6291464 | tf_op jit(solution)/shard_map/ppermute | solution.py:391
  46.8 32.9 %collective-permute-start.8 = (bf16[128,2048]{1,0:T(8,128)(2,1)S(1)}, bf16[128,2048]{1,0:T(8,128)(2,1)}, u32[]{:S(2)}, u32[]{:S(2)}) collective-permute-start(bf16[128,2048]{1,0:T(8,128)(2,1)S(1)} %collective-permute-done.7.refs_0_), channel_id=1, source_target_pairs={{0,1},{1,0},{2,3},{3,2},{4,5},{5,4},{6,7},{7,6},{8,9},{9,8},{10,11... | collective-permute-start | bytes 1572872 | tf_op jit(solution)/shard_map/ppermute | solution.py:391
  56.1 23.6 %collective-permute-start.10 = (bf16[128,2048]{1,0:T(8,128)(2,1)}, bf16[128,2048]{1,0:T(8,128)(2,1)}, u32[]{:S(2)}, u32[]{:S(2)}) collective-permute-start(bf16[128,2048]{1,0:T(8,128)(2,1)} %collective-permute-done.9.refs_2_), channel_id=1, source_target_pairs={{0,1},{1,0},{2,3},{3,2},{4,5},{5,4},{6,7},{7,6},{8,9},{9,8},{10,11... | collective-permute-start | bytes 1572872 | tf_op jit(solution)/shard_map/ppermute | solution.py:391
  56.9 29.6 %collective-permute-start.12 = (bf16[128,2048]{1,0:T(8,128)(2,1)}, bf16[128,2048]{1,0:T(8,128)(2,1)S(1)}, u32[]{:S(2)}, u32[]{:S(2)}) collective-permute-start(bf16[128,2048]{1,0:T(8,128)(2,1)} %collective-permute-done.11.refs_0_), channel_id=1, source_target_pairs={{0,1},{1,0},{2,3},{3,2},{4,5},{5,4},{6,7},{7,6},{8,9},{9,8},{10,11... | collective-permute-start | bytes 1572872 | tf_op jit(solution)/shard_map/ppermute | solution.py:391
  65.6 20.9 %collective-permute-start.14 = (bf16[128,2048]{1,0:T(8,128)(2,1)}, bf16[128,2048]{1,0:T(8,128)(2,1)}, u32[]{:S(2)}, u32[]{:S(2)}) collective-permute-start(bf16[128,2048]{1,0:T(8,128)(2,1)} %collective-permute-done.13.refs_2_), channel_id=1, source_target_pairs={{0,1},{1,0},{2,3},{3,2},{4,5},{5,4},{6,7},{7,6},{8,9},{9,8},{10,11... | collective-permute-start | bytes 1572872 | tf_op jit(solution)/shard_map/ppermute | solution.py:391
  112.9 5.0 %collective-permute-start.15 = (bf16[2,128,256]{2,1,0:T(8,128)(2,1)}, bf16[2,128,256]{2,1,0:T(8,128)(2,1)S(1)}, u32[]{:S(2)}, u32[]{:S(2)}) collective-permute-start(bf16[2,128,256]{2,1,0:T(8,128)(2,1)} %get-tuple-element.14), channel_id=1, source_target_pairs={{0,1},{1,0},{2,3},{3,2},{4,5},{5,4},{6,7},{7,6},{8,9},{9,8},{10,11... | collective-permute-start | bytes 393224 | tf_op jit(solution)/shard_map/ppermute | solution.py:399
  113.5 9.9 %collective-permute-start.16 = (bf16[2,128,256]{2,1,0:T(8,128)(2,1)}, bf16[2,128,256]{2,1,0:T(8,128)(2,1)S(1)}, u32[]{:S(2)}, u32[]{:S(2)}) collective-permute-start(bf16[2,128,256]{2,1,0:T(8,128)(2,1)} %get-tuple-element.15), channel_id=1, source_target_pairs={{0,4},{1,5},{2,6},{3,7},{4,0},{5,1},{6,2},{7,3},{8,12},{9,13},{10,... | collective-permute-start | bytes 393224 | tf_op jit(solution)/shard_map/ppermute | solution.py:399
  113.5 10.9 %collective-permute-start.17 = (bf16[2,128,256]{2,1,0:T(8,128)(2,1)}, bf16[2,128,256]{2,1,0:T(8,128)(2,1)S(1)}, u32[]{:S(2)}, u32[]{:S(2)}) collective-permute-start(bf16[2,128,256]{2,1,0:T(8,128)(2,1)} %get-tuple-element.16), channel_id=1, source_target_pairs={{0,5},{1,4},{2,7},{3,6},{4,1},{5,0},{6,3},{7,2},{8,13},{9,12},{10,... | collective-permute-start | bytes 393224 | tf_op jit(solution)/shard_map/ppermute | solution.py:399
  114.9 9.5 %collective-permute-start.18 = (bf16[2,128,256]{2,1,0:T(8,128)(2,1)}, bf16[2,128,256]{2,1,0:T(8,128)(2,1)S(1)}, u32[]{:S(2)}, u32[]{:S(2)}) collective-permute-start(bf16[2,128,256]{2,1,0:T(8,128)(2,1)} %get-tuple-element.17), channel_id=1, source_target_pairs={{0,8},{1,9},{2,10},{3,11},{4,12},{5,13},{6,14},{7,15},{8,0},{9,1},... | collective-permute-start | bytes 393224 | tf_op jit(solution)/shard_map/ppermute | solution.py:399
  116.4 19.6 %collective-permute-start.19 = (bf16[2,128,256]{2,1,0:T(8,128)(2,1)}, bf16[2,128,256]{2,1,0:T(8,128)(2,1)S(1)}, u32[]{:S(2)}, u32[]{:S(2)}) collective-permute-start(bf16[2,128,256]{2,1,0:T(8,128)(2,1)} %get-tuple-element.18), channel_id=1, source_target_pairs={{0,9},{1,8},{2,11},{3,10},{4,13},{5,12},{6,15},{7,14},{8,1},{9,0},... | collective-permute-start | bytes 393224 | tf_op jit(solution)/shard_map/ppermute | solution.py:399
  117.9 18.1 %copy-start.9 = (bf16[2,128,256]{2,1,0:T(8,128)(2,1)}, bf16[2,128,256]{2,1,0:T(8,128)(2,1)S(1)}, u32[]{:S(2)}) copy-start(bf16[2,128,256]{2,1,0:T(8,128)(2,1)S(1)} %collective-permute-done.15.refs_1_) | copy-start | bytes 393220
  117.9 18.1 %collective-permute-start.20 = (bf16[2,128,256]{2,1,0:T(8,128)(2,1)}, bf16[2,128,256]{2,1,0:T(8,128)(2,1)S(1)}, u32[]{:S(2)}, u32[]{:S(2)}) collective-permute-start(bf16[2,128,256]{2,1,0:T(8,128)(2,1)} %get-tuple-element.19), channel_id=1, source_target_pairs={{0,12},{1,13},{2,14},{3,15},{4,8},{5,9},{6,10},{7,11},{8,4},{9,5},... | collective-permute-start | bytes 393224 | tf_op jit(solution)/shard_map/ppermute | solution.py:399
  123.4 12.6 %collective-permute-start.21 = (bf16[2,128,256]{2,1,0:T(8,128)(2,1)}, bf16[2,128,256]{2,1,0:T(8,128)(2,1)S(1)}, u32[]{:S(2)}, u32[]{:S(2)}) collective-permute-start(bf16[2,128,256]{2,1,0:T(8,128)(2,1)} %get-tuple-element.20), channel_id=1, source_target_pairs={{0,13},{1,12},{2,15},{3,14},{4,9},{5,8},{6,11},{7,10},{8,5},{9,4},... | collective-permute-start | bytes 393224 | tf_op jit(solution)/shard_map/ppermute | solution.py:399
  143.3 25.7 %collective-permute-start.23 = (bf16[256,2048]{1,0:T(8,128)(2,1)}, bf16[256,2048]{1,0:T(8,128)(2,1)S(1)}, u32[]{:S(2)}, u32[]{:S(2)}) collective-permute-start(bf16[256,2048]{1,0:T(8,128)(2,1)} %mix_1.1), channel_id=1, source_target_pairs={{0,2},{1,3},{2,0},{3,1},{4,6},{5,7},{6,4},{7,5},{8,10},{9,11},{10,... | collective-permute-start | bytes 3145736 | tf_op jit(solution)/shard_map/ppermute | solution.py:391
  (9 other events, 57.6 us)
